TPU v7x, 768 devices: a whole 4x8x12 slice. The times are simulated.
768 devices in a mesh: sp: 16 (over y, core), tp: 48 (over z, x).
Axes of the slice: x: 4, y: 8, z: 12, core: 2. Of those that a mesh axis runs over, the one named last changes fastest.
Arguments:
- queries: bfloat16 [2048, 3072], P('sp'), may hold values from -6 to 6
- attn_out: bfloat16 [2048, 3072], P('sp'), may hold values from -3 to 3
- log_norm: float32 [2048, 12], P('sp'), as said below
- cotangent: bfloat16 [2048, 3072], P('sp'), may hold values from -96 to 96
- keys: bfloat16 [24576, 512], P(('sp', 'tp')), may hold values from -6 to 6
- values: bfloat16 [24576, 512], P(('sp', 'tp')), may hold values from -6 to 6
- source: bfloat16 [24576, 3072], P('sp', 'tp'), may hold values from -6 to 6
- w_query: bfloat16 [3072, 3072], P('tp'), may hold values from -0.109375 to 0.109375
- w_key: bfloat16 [3072, 512], P('tp'), may hold values from -0.109375 to 0.109375
- w_value: bfloat16 [3072, 512], P('tp'), may hold values from -0.109375 to 0.109375
Outputs:
- d_target: bfloat16 [2048, 3072], P('sp', 'tp')
- d_source: bfloat16 [24576, 3072], P('sp', 'tp')
- d_wvalue: float32 [3072, 512], P('tp')
Inputs may be any that keep to these rules, and one draw needn't show every extreme that they name: `log_norm`: the logarithm of the softmax total saved by the forward pass, near log(24576) + 0.5.
All inputs are finite; a program needn't handle non-finite values.
Results may differ from a plain program's by a relative error of at most 0.024.
Values may be sent and summed in bfloat16 or wider, within the bound.
A program may use at most 32 MiB of HBM per device.

v0:
```python
import math

import jax
import jax.numpy as jnp
from jax import lax
from jax.sharding import Mesh
from jax.sharding import PartitionSpec as P

HEADS = 12
KV_HEADS = 2
HEAD_DIM = 256
TP = ("tp_0", "tp_1")
SP_TP = ("sp", "tp_0", "tp_1")


def cut_along(array, dim, size):
    lengths = array.shape
    parts = array.reshape(*lengths[:dim], size, lengths[dim] // size, *lengths[dim + 1 :])
    return jnp.moveaxis(parts, dim, 0)


def sum_at_owner(array, axis, dim):
    parts = cut_along(array, dim, lax.axis_size(axis))
    arrived = lax.all_to_all(parts, axis, split_axis=0, concat_axis=0, tiled=True)
    return arrived.astype(jnp.float32).sum(axis=0)


def sent_together(arrays, axis, dim, along):
    both = jnp.concatenate(arrays, axis=along)
    out, at, gathered = (sum_at_owner(both, axis, dim), 0, [])
    for a in arrays:
        gathered.append(lax.slice_in_dim(out, at, at + a.shape[along], axis=along))
        at += a.shape[along]
    return tuple(gathered)


def whole_of(array, axes, dim):
    out = array
    for number in range(len(axes) - 1, -1, -1):
        out = lax.all_gather(out, axes[number], axis=dim, tiled=True)
    return out


def from_everyone(array, axis):
    size = lax.axis_size(axis)
    return lax.all_to_all(
        jnp.broadcast_to(array[None], (size, *array.shape)), axis, 0, 0, tiled=True
    )


def taken_together(array, axis):
    return from_everyone(array, axis).astype(jnp.float32).sum(axis=0)


def laid_out(parts, dim):
    lengths = list(parts.shape[1:])
    lengths[dim] *= parts.shape[0]
    return jnp.moveaxis(parts, 0, dim).reshape(lengths)


def collect(array, axis, dim):
    parts = from_everyone(array, axis)
    return laid_out(parts, dim)


def shards(queries, attn_out, log_norm, cotangent, keys, values, source, w_query, w_key, w_value):
    single_precision = jnp.float32
    repeat = HEADS // KV_HEADS
    score_scale = 1.0 / math.sqrt(HEAD_DIM)
    rows = queries.shape[0]
    near_keys, near_values = (
        lax.all_gather(keys, "sp", axis=0, tiled=True),
        lax.all_gather(values, "sp", axis=0, tiled=True),
    )
    span = near_keys.shape[0]
    query_tensor4 = queries.reshape(rows, KV_HEADS, repeat, HEAD_DIM)
    output_gradient4 = cotangent.reshape(rows, KV_HEADS, repeat, HEAD_DIM)
    out4 = attn_out.reshape(rows, KV_HEADS, repeat, HEAD_DIM)
    shared_key_heads = near_keys.reshape(span, KV_HEADS, HEAD_DIM)
    shared_value_heads = near_values.reshape(span, KV_HEADS, HEAD_DIM)
    delta = jnp.sum(
        output_gradient4.astype(single_precision) * out4.astype(single_precision), axis=3
    )
    delta = jnp.transpose(delta, (1, 2, 0))[..., None]
    lse = jnp.transpose(log_norm.reshape(rows, KV_HEADS, repeat), (1, 2, 0))[..., None]
    logit_scores = (
        jnp.einsum(
            "znjk,wnk->njzw",
            query_tensor4,
            shared_key_heads,
            preferred_element_type=single_precision,
        )
        * score_scale
    )
    probs = jnp.exp(logit_scores - lse)
    probabilities16 = probs.astype(jnp.bfloat16)
    prob_gradient = jnp.einsum(
        "znjk,wnk->njzw",
        output_gradient4,
        shared_value_heads,
        preferred_element_type=single_precision,
    )
    score_gradient = (probs * (prob_gradient - delta)).astype(jnp.bfloat16)
    query_gradient_piece = (
        jnp.einsum(
            "wohn,nwb->hwob",
            score_gradient,
            shared_key_heads,
            preferred_element_type=single_precision,
        )
        * score_scale
    )
    query_gradient_piece = query_gradient_piece.reshape(rows, -1)
    key_gradient_piece = (
        jnp.einsum(
            "nkjv,jnka->vna", score_gradient, query_tensor4, preferred_element_type=single_precision
        )
        * score_scale
    )
    value_gradient_piece = jnp.einsum(
        "nkjv,jnka->vna", probabilities16, output_gradient4, preferred_element_type=single_precision
    )
    own_keys, own_values = sent_together(
        (
            key_gradient_piece.reshape(span, -1).astype(jnp.bfloat16),
            value_gradient_piece.reshape(span, -1).astype(jnp.bfloat16),
        ),
        "sp",
        0,
        1,
    )
    stacked = jnp.concatenate(
        [own_keys.astype(jnp.bfloat16), own_values.astype(jnp.bfloat16)], axis=1
    )
    group = whole_of(stacked, TP, 0)
    weights = jnp.concatenate([w_key, w_value], axis=1)
    d_source = lax.dot_general(
        group, weights, (((1,), (1,)), ((), ())), preferred_element_type=single_precision
    ).astype(jnp.bfloat16)
    kv_width = w_value.shape[1]
    weight_term = lax.dot_general(
        source,
        group[:, kv_width:],
        (((0,), (0,)), ((), ())),
        preferred_element_type=single_precision,
    )
    d_wvalue = taken_together(weight_term.astype(jnp.bfloat16), "sp").astype(jnp.float32)
    column_block = sum_at_owner(query_gradient_piece.astype(jnp.bfloat16), TP, 1).astype(
        jnp.bfloat16
    )
    dq16 = collect(column_block, TP, 1)
    d_target = lax.dot_general(
        dq16, w_query, (((1,), (1,)), ((), ())), preferred_element_type=single_precision
    ).astype(jnp.bfloat16)
    return (d_target, d_source, d_wvalue)


def solution(mesh):
    split = Mesh(mesh.devices.reshape(mesh.shape["sp"], 12, 4), ("sp", "tp_0", "tp_1"))
    in_specs = (
        P("sp", None),
        P("sp", None),
        P("sp", None),
        P("sp", None),
        P(SP_TP, None),
        P(SP_TP, None),
        P("sp", TP),
        P(TP, None),
        P(TP, None),
        P(TP, None),
    )
    out_specs = (P("sp", TP), P("sp", TP), P(TP, None))
    return jax.shard_map(
        shards, mesh=split, in_specs=in_specs, out_specs=out_specs, check_vma=False
    )
```

profile of v0, /device:TPU:1, one launch (start us, length us, event | category | flops | bytes accessed | tf_op | source)
XLA Modules:
  0.0 258.6 jit_solution(2164256492844210666)
XLA Ops:
  7.2 0.0 copy-start
  7.2 0.0 copy-start.4
  7.2 0.0 copy-start.6
  7.2 0.0 copy-start.5
  7.2 0.0 all-gather.2.cloned.1.call-start
  7.3 26.4 %all_gather.12 = bf16[512,512]{1,0:T(8,128)(2,1)S(1)} all-gather(bf16[32,512]{1,0:T(8,128)(2,1)} %param.14), channel_id=1, replica_groups=mesh['sp'=16,'tp_0'=12,'tp_1'=4] {'sp'}, dimensions={0}, use_global_device_ids=true | all-gather | bytes 557056 | tf_op jit(solution)/shard_map/all_gather | solution.py:72
  33.7 0.2 copy.50
  33.9 1.5 copy.51
  35.4 0.0 copy-done.4
  35.4 0.4 copy.55
  35.8 1.5 copy.58
  37.3 0.0 copy-done.6
  37.3 0.0 copy-done.5
  37.3 18.8 %all_gather.13 = bf16[512,512]{1,0:T(8,128)(2,1)} all-gather(bf16[32,512]{1,0:T(8,128)(2,1)S(1)} %copy-done.5), channel_id=1, replica_groups=mesh['sp'=16,'tp_0'=12,'tp_1'=4] {'sp'}, dimensions={0}, use_global_device_ids=true | all-gather | bytes 557056 | tf_op jit(solution)/shard_map/all_gather | solution.py:73
  56.1 2.0 copy.54
  58.2 0.6 fusion.35
  58.8 0.0 copy-start.2
  58.8 0.2 fusion.8
  59.0 0.7 fusion.20
  59.7 0.1 copy-done.2
  59.8 1.0 fusion.1
  60.8 0.0 copy-start.3
  60.8 0.6 fusion.23
  61.5 0.5 copy-done.3
  62.0 0.5 copy.63
  62.5 0.3 convert_element_type.77
  62.9 0.5 copy.65
  63.4 0.3 convert_element_type.81
  63.8 0.1 pad_maximum_fusion
  63.9 32.0 %all_to_all.20 = bf16[16,32,1024]{2,1,0:T(8,128)(2,1)S(1)} all-to-all(bf16[16,32,1024]{2,1,0:T(8,128)(2,1)S(1)} %pad_maximum_fusion), channel_id=1, replica_groups=mesh['sp'=16,'tp_0'=12,'tp_1'=4] {'sp'}, dimensions={0} | all-to-all | bytes 2097152 | tf_op jit(solution)/shard_map/all_to_all | solution.py:24
  95.9 0.2 reduce.1
  96.1 10.6 %all_gather.14 = bf16[128,1024]{1,0:T(8,128)(2,1)} all-gather(bf16[32,1024]{1,0:T(8,128)(2,1)S(1)} %reduce.1), channel_id=1, replica_groups=mesh['sp'=16,'tp_0'=12,'tp_1'=4] {'tp_1'}, dimensions={0}, use_global_device_ids=true | all-gather | bytes 327680 | tf_op jit(solution)/shard_map/all_gather | solution.py:40
  106.7 0.0 all-gather.2.cloned.1.call-update
  106.7 2.1 fusion.19
  108.9 0.4 copy.61
  109.3 46.5 %all_to_all.21 = bf16[48,128,64]{1,2,0:T(8,128)(2,1)S(1)} all-to-all(bf16[48,128,64]{1,2,0:T(8,128)(2,1)S(1)} %bitcast.87), channel_id=1, replica_groups=mesh['sp'=16,'tp_0'=12,'tp_1'=4] {'tp_0','tp_1'}, dimensions={0} | all-to-all | bytes 1572864 | tf_op jit(solution)/shard_map/all_to_all | solution.py:24
  155.8 0.1 reduce_sum.40
  155.9 1.1 broadcast_in_dim.4
  157.0 12.0 %all-to-all-start.1 = ((bf16[48,128,64]{1,2,0:T(8,128)(2,1)}), bf16[48,128,64]{1,2,0:T(8,128)(2,1)}, u32[]{:S(2)}, u32[]{:S(2)}) async-start(bf16[48,128,64]{1,2,0:T(8,128)(2,1)} %broadcast_in_dim.4), calls=%async_computation.1 | async-start | bytes 1572864 | tf_op jit(solution)/shard_map/all_to_all | solution.py:46
  169.0 40.3 %all-gather.2.cloned.1.call-done = bf16[1536,1024]{1,0:T(8,128)(2,1)} async-done(((bf16[128,1024]{1,0:T(8,128)(2,1)}), bf16[1536,1024]{1,0:T(8,128)(2,1)}) %all-gather.2.cloned.1.call-update) | async-done | bytes 3145744 | tf_op jit(solution)/shard_map/all_gather | solution.py:40
  209.3 0.0 copy-start.1
  209.3 2.7 %fusion.27 = bf16[64,512]{1,0:T(8,128)(2,1)} fusion(bf16[1536,64]{0,1:T(8,128)(2,1)} %param.16, bf16[1536,1024]{1,0:T(8,128)(2,1)} %all-gather.2.cloned.1.call-done), kind=kOutput, calls=%fused_computation.25 | convolution fusion | flops 100696064 | bytes 1835008 | tf_op jit(solution)/shard_map/dot_general | solution.py:141
  212.0 0.0 all-to-all-done.1
  212.0 1.9 broadcast_in_dim.5
  213.9 7.7 %all-to-all-start.3 = ((bf16[16,64,512]{2,1,0:T(8,128)(2,1)}), bf16[16,64,512]{2,1,0:T(8,128)(2,1)}, u32[]{:S(2)}, u32[]{:S(2)}) async-start(bf16[16,64,512]{2,1,0:T(8,128)(2,1)} %broadcast_in_dim.5), calls=%async_computation.3 | async-start | bytes 2097152 | tf_op jit(solution)/shard_map/all_to_all | solution.py:46
  221.6 0.0 copy-done
  221.6 2.0 convolution_convert_fusion.1
  223.6 0.0 copy-done.1
  223.6 2.6 %convolution_convert_fusion = bf16[1536,64]{0,1:T(8,128)(2,1)} fusion(bf16[1536,1024]{1,0:T(8,128)(2,1)S(1)} %copy-done.1, bf16[64,512]{1,0:T(8,128)(2,1)} %param.19, bf16[64,512]{1,0:T(8,128)(2,1)} %param.18), kind=kOutput, calls=%fused_computation.6 | convolution fusion | flops 201687040 | bytes 3473408 | tf_op jit(solution)/shard_map/dot_general | solution.py:137
  226.2 23.5 %all-to-all-done.3 = bf16[16,64,512]{2,1,0:T(8,128)(2,1)} async-done(((bf16[16,64,512]{2,1,0:T(8,128)(2,1)}), bf16[16,64,512]{2,1,0:T(8,128)(2,1)}, u32[]{:S(2)}, u32[]{:S(2)}) %all-to-all-start.3) | async-done | bytes 1048608 | tf_op jit(solution)/shard_map/all_to_all | solution.py:46
  249.8 2.0 convert_reduce_fusion
  (1 shorter events, 0.0 us)
Async XLA Ops:
  7.2 214.4 %copy-start = (bf16[64,3072]{1,0:T(8,128)(2,1)S(1)}, bf16[64,3072]{1,0:T(8,128)(2,1)}, u32[]{:S(2)}) copy-start(bf16[64,3072]{1,0:T(8,128)(2,1)} %param.17) | copy-start | bytes 1179652
  7.2 28.2 %copy-start.4 = (bf16[128,3072]{1,0:T(8,128)(2,1)S(1)}, bf16[128,3072]{1,0:T(8,128)(2,1)}, u32[]{:S(2)}) copy-start(bf16[128,3072]{1,0:T(8,128)(2,1)} %param.13) | copy-start | bytes 2359300
  7.2 30.1 %copy-start.6 = (f32[128,12]{0,1:T(8,128)S(1)}, f32[128,12]{0,1:T(8,128)}, u32[]{:S(2)}) copy-start(f32[128,12]{0,1:T(8,128)} %param.12) | copy-start | bytes 18436
  7.2 30.1 %copy-start.5 = (bf16[32,512]{1,0:T(8,128)(2,1)S(1)}, bf16[32,512]{1,0:T(8,128)(2,1)}, u32[]{:S(2)}) copy-start(bf16[32,512]{1,0:T(8,128)(2,1)} %param.15) | copy-start | bytes 98308
  7.2 202.1 %all-gather.2.cloned.1.call-start = ((), (), s32[]{:S(2)}) async-start(), calls=%async_computation.4 | async-start | bytes 3407872 | tf_op jit(solution)/shard_map/all_gather | solution.py:40
  58.8 1.0 copy-start.2
  60.8 1.2 copy-start.3
  157.0 55.0 %all-to-all-start.1 = ((bf16[48,128,64]{1,2,0:T(8,128)(2,1)}), bf16[48,128,64]{1,2,0:T(8,128)(2,1)}, u32[]{:S(2)}, u32[]{:S(2)}) async-start(bf16[48,128,64]{1,2,0:T(8,128)(2,1)} %broadcast_in_dim.4), calls=%async_computation.1 | async-start | bytes 1572864 | tf_op jit(solution)/shard_map/all_to_all | solution.py:46
  209.3 14.3 %copy-start.1 = (bf16[1536,1024]{1,0:T(8,128)(2,1)S(1)}, bf16[1536,1024]{1,0:T(8,128)(2,1)}, u32[]{:S(2)}) copy-start(bf16[1536,1024]{1,0:T(8,128)(2,1)} %all-gather.2.cloned.1.call-done) | copy-start | bytes 9437188
  213.9 35.8 %all-to-all-start.3 = ((bf16[16,64,512]{2,1,0:T(8,128)(2,1)}), bf16[16,64,512]{2,1,0:T(8,128)(2,1)}, u32[]{:S(2)}, u32[]{:S(2)}) async-start(bf16[16,64,512]{2,1,0:T(8,128)(2,1)} %broadcast_in_dim.5), calls=%async_computation.3 | async-start | bytes 2097152 | tf_op jit(solution)/shard_map/all_to_all | solution.py:46
Sparse Core Ops, SparseCore 0:
  106.9 102.4 all-gather.1
where the time goes:
time: 259 us
  blocking collectives  134 us (52%)
  waiting for transfers between devices  63.9 us (25%)
  starting transfers between devices  19.7 us (8%)
  between operations  14.2 us (5%)
  matrix products  12.3 us (5%)
  local copies, waits for them, and re-layouts  11.4 us (4%)
  other arithmetic  2.7 us (1%)
    all_to_all x2, blocking collectives, sum_at_owner(): lax.all_to_all(parts, axis, split_axis=0, concat_axis=0, tiled=True)  78.6 us
    all_gather x1, waiting for transfers between devices, whole_of(): out = lax.all_gather(out, axes[number], axis=dim, tiled=True)  40.3 us
    all_gather x1, blocking collectives, shards(): lax.all_gather(keys, 'sp', axis=0, tiled=True)  26.4 us
    all_to_all x2, waiting for transfers between devices, from_everyone(): lax.all_to_all(jnp.broadcast_to(array[None], (size, *array.shape)), axis,...  23.5 us
    all_to_all x2, starting transfers between devices, from_everyone(): lax.all_to_all(jnp.broadcast_to(array[None], (size, *array.shape)), axis,...  19.7 us
    all_gather x1, blocking collectives, shards(): lax.all_gather(values, 'sp', axis=0, tiled=True)  18.8 us
    all_gather x1, blocking collectives, whole_of(): out = lax.all_gather(out, axes[number], axis=dim, tiled=True)  10.6 us
  transfers between devices with their start and end apart: 3, of which 2 were waited for; matrix products, arithmetic and copies ran while one was open for 4% of the time, Pallas kernels for 0%

commit v1 on v0

v1 whole, which is shorter than its diff:
```python
import math

import jax
import jax.numpy as jnp
from jax import lax
from jax.experimental import pallas as pl
from jax.experimental.pallas import tpu as pltpu
from jax.sharding import Mesh
from jax.sharding import PartitionSpec as P

HEADS = 12
KV_HEADS = 2
HEAD_DIM = 256
PER_GROUP = HEADS // KV_HEADS
NY, NC, NZ, NX = 8, 2, 12, 4
MESH = pl.DeviceIdType.MESH
F32 = jnp.float32
BF16 = jnp.bfloat16
NT = (((1,), (1,)), ((), ()))
TN = (((0,), (0,)), ((), ()))
NN = (((1,), (0,)), ((), ()))
Y_CHAINS = ((0, 1, 4), (1, -1, 4), (1, 1, 3), (0, -1, 3))
Z_CHAINS = ((0, 1, 6), (1, -1, 6), (1, 1, 5), (0, -1, 5))
COPIES = 176


def mm(a, b, dims):
    return lax.dot_general(a, b, dims, preferred_element_type=F32)


def kernel(
    q_ref, o_ref, do_ref, lse_ref, kv_ref, src_ref, wkv_ref, wq_ref,
    dt_ref, ds_ref, dw_ref,
    kv, qs, dos, delta, dq_acc, part, from_core, paired, ring_in, ring_out, own,
    dqp, x_in, x_sum, z_in, chunk, gathered, dq_all,
    wkv, wq, sx, wvp, wv_in, sums, sum_in, total, totals,
    dst_part, dst_in, dtp, dt_in,
    send_sem, recv_sem,
):
    y, c, z, x = (lax.axis_index(a) for a in ("y", "c", "z", "x"))
    scale = 1.0 / math.sqrt(HEAD_DIM)
    made = []

    def step(v, d, n):
        return lax.rem(v + d + n, n)

    def remote(src, dst, **where):
        number = len(made)
        copy = pltpu.make_async_remote_copy(
            src_ref=src,
            dst_ref=dst,
            send_sem=send_sem.at[number],
            recv_sem=recv_sem.at[number],
            device_id=where,
            device_id_type=MESH,
        )
        copy.start()
        made.append(copy)
        return copy

    barrier = pltpu.get_barrier_semaphore()
    peers = [{"y": step(y, 1, NY)}, {"y": step(y, -1, NY)}, {"c": 1 - c}]
    peers += [{"x": step(x, d, NX)} for d in range(1, NX)]
    peers += [{"z": step(z, d, NZ)} for d in range(1, NZ)]
    for peer in peers:
        pl.semaphore_signal(barrier, inc=1, device_id=peer, device_id_type=MESH)
    pl.semaphore_wait(barrier, len(peers))

    hops = {}
    for n, (w, d, length) in enumerate(Y_CHAINS):
        hops[n] = remote(kv_ref.at[w], kv.at[y, c, w], y=step(y, d, NY))
    to_core = [remote(kv_ref.at[w], kv.at[y, c, w], c=1 - c) for w in range(2)]
    x_src = [remote(src_ref.at[:, step(x, d, NX)], sx.at[x], x=step(x, d, NX)) for d in range(1, NX)]
    x_wkv = [remote(wkv_ref.at[c], wkv.at[x, c], x=step(x, d, NX)) for d in range(1, NX)]

    kv[y, c] = kv_ref[...]
    wkv[x] = wkv_ref[...]
    wq[x] = wq_ref[...]
    for xx in range(NX):
        @pl.when(x == xx)
        def _():
            sx[xx] = src_ref[:, xx]
    for g in range(KV_HEADS):
        for h in range(PER_GROUP):
            columns = slice((g * PER_GROUP + h) * HEAD_DIM, (g * PER_GROUP + h + 1) * HEAD_DIM)
            rows = slice(h * 128, (h + 1) * 128)
            qs[g, rows] = q_ref[:, columns]
            dos[g, rows] = do_ref[:, columns]
            prod = do_ref[:, columns].astype(F32) * o_ref[:, columns].astype(F32)
            halves = prod[:, :128] + prod[:, 128:]
            delta[g, :, rows] = jnp.sum(jnp.transpose(halves), axis=0, keepdims=True)

    for h in range(1, 5):
        for n, (w, d, length) in enumerate(Y_CHAINS):
            if h > length:
                continue
            hops[n].wait_recv()
            at = kv.at[step(y, -d * h, NY), c, w]
            if h < length:
                hops[n] = remote(at, at, y=step(y, d, NY))
            to_core.append(remote(at, at, c=1 - c))
    for copy in to_core:
        copy.wait_recv()

    ROWS = 256
    for g in range(KV_HEADS):
        cols = slice(g * HEAD_DIM, (g + 1) * HEAD_DIM)

        def block(n, carry, g=g, cols=cols):
            base = n * (ROWS // 64)
            kb = kv[pl.ds(base, ROWS // 64), :, 0, :, cols].reshape(ROWS, HEAD_DIM)
            vb = kv[pl.ds(base, ROWS // 64), :, 1, :, cols].reshape(ROWS, HEAD_DIM)
            scores = mm(kb, qs[g], NT) * scale
            probs = jnp.exp(scores - lse_ref[g])
            dprob = mm(vb, dos[g], NT)
            dscore = (probs * (dprob - delta[g])).astype(BF16)
            dk = (mm(dscore, qs[g], NN) * scale).astype(BF16)
            dv = mm(probs.astype(BF16), dos[g], NN).astype(BF16)
            term = mm(dscore, kb, TN) * scale
            dq_acc[g] = jnp.where(n == 0, term, dq_acc[g] + term)
            for yy in range(ROWS // 64):
                for cc in range(NC):
                    at = slice((yy * 2 + cc) * 32, (yy * 2 + cc + 1) * 32)
                    part[cc, base + yy, 0, :, cols] = dk[at]
                    part[cc, base + yy, 1, :, cols] = dv[at]
            return carry

        lax.fori_loop(0, 512 // ROWS, block, 0)
    for g in range(KV_HEADS):
        for h in range(PER_GROUP):
            for xx in range(NX):
                at = h * 128 + xx * 32
                dqp[xx, g * PER_GROUP + h] = dq_acc[g, at : at + 32].astype(BF16)

    order = (4, 3, -3, 2, -2, 1, -1, 0)
    core_in = {d: remote(part.at[1 - c, step(y, d, NY)], from_core.at[step(y, d, NY)], c=1 - c) for d in order}
    x_dq = [remote(dqp.at[step(x, d, NX)], x_in.at[d - 1], x=step(x, d, NX)) for d in range(1, NX)]
    x_wq = [remote(wq_ref.at[c], wq.at[x, c], x=step(x, d, NX)) for d in range(1, NX)]
    for d in range(1, NX):
        x_wkv[d - 1].wait_recv()
    c_wkv = [remote(wkv.at[step(x, -d, NX), c], wkv.at[step(x, -d, NX), c], c=1 - c) for d in range(1, NX)]

    for d in order:
        core_in[d].wait_recv()
        at = step(y, d, NY)
        paired[at] = (part[c, at].astype(F32) + from_core[at].astype(F32)).astype(BF16)

    for n, (w, d, length) in enumerate(Y_CHAINS):
        hops[n] = remote(paired.at[step(y, d * length, NY), w], ring_in.at[n, 0], y=step(y, d, NY))

    def sum_over_x():
        for d in range(1, NX):
            x_dq[d - 1].wait_recv()
        for hh in range(NZ):
            total_rows = dqp[x, hh].astype(F32)
            for d in range(1, NX):
                total_rows += x_in[d - 1, hh].astype(F32)
            x_sum[hh] = total_rows.astype(BF16)
        return [remote(x_sum.at[step(z, d, NZ)], z_in.at[d - 1], z=step(z, d, NZ)) for d in range(1, NZ)]

    for h in range(1, 5):
        for n, (w, d, length) in enumerate(Y_CHAINS):
            if h > length:
                continue
            hops[n].wait_recv()
            if h < length:
                ring_out[n, h - 1] = (
                    ring_in[n, h - 1].astype(F32) + paired[step(y, d * (length - h), NY), w].astype(F32)
                ).astype(BF16)
                hops[n] = remote(ring_out.at[n, h - 1], ring_in.at[n, h], y=step(y, d, NY))
        if h == 3:
            z_dq = sum_over_x()
    last = {(w, d): ring_in.at[n, length - 1] for n, (w, d, length) in enumerate(Y_CHAINS)}
    for w in range(2):
        own[w] = (
            paired[y, w].astype(F32) + last[w, 1][...].astype(F32) + last[w, -1][...].astype(F32)
        ).astype(BF16)

    for n, (w, d, length) in enumerate(Z_CHAINS):
        hops[n] = remote(own.at[w], gathered.at[w, z], z=step(z, d, NZ))
    for w in range(2):
        gathered[w, z] = own[w]

    def over_z(h):
        for n, (w, d, length) in enumerate(Z_CHAINS):
            if h > length:
                continue
            hops[n].wait_recv()
            if h < length:
                at = gathered.at[w, step(z, -d * h, NZ)]
                hops[n] = remote(at, at, z=step(z, d, NZ))

    over_z(1)
    over_z(2)
    for copy in z_dq:
        copy.wait_recv()
    rows32 = x_sum[z].astype(F32)
    for d in range(1, NZ):
        rows32 += z_in[d - 1].astype(F32)
    chunk[...] = rows32.astype(BF16)
    z_dq_all = [remote(chunk, dq_all.at[z], z=step(z, d, NZ)) for d in range(1, NZ)]
    dq_all[z] = chunk[...]
    over_z(3)
    over_z(4)
    for d in range(1, NX):
        x_wq[d - 1].wait_recv()
    c_wq = [remote(wq.at[step(x, -d, NX), c], wq.at[step(x, -d, NX), c], c=1 - c) for d in range(1, NX)]
    over_z(5)
    over_z(6)

    dv_rows = gathered[1].reshape(NZ * 32, 512)
    for d in range(1, NX):
        x_src[d - 1].wait_recv()
    for xx in range(NX):
        wvp[xx] = mm(sx[xx].reshape(NZ * 32, 64), dv_rows, TN).astype(BF16)
    x_wv = [remote(wvp.at[step(x, d, NX)], wv_in.at[d - 1], x=step(x, d, NX)) for d in range(1, NX)]
    for d in range(1, NX):
        c_wkv[d - 1].wait_recv()
    dk_rows = gathered[0].reshape(NZ * 32, 512)
    weights = wkv[...]
    w_key = weights[:, :, 0].reshape(NX * 64, 512)
    w_value = weights[:, :, 1].reshape(NX * 64, 512)
    grad = mm(w_key, dk_rows, NT) + mm(w_value, dv_rows, NT)
    for xx in range(NX):
        dst_part[xx] = grad[xx * 64 : (xx + 1) * 64].astype(BF16)
    x_ds = [remote(dst_part.at[step(x, d, NX)], dst_in.at[x], x=step(x, d, NX)) for d in range(1, NX)]
    dst_in[x] = dst_part[x]

    for copy in x_wv:
        copy.wait_recv()
    w_sum = wvp[x].astype(F32)
    for d in range(1, NX):
        w_sum += wv_in[d - 1].astype(F32)
    for j in range(16):
        sums[j] = w_sum[(j // 4) * 16 : (j // 4 + 1) * 16, (j % 4) * 128 : (j % 4 + 1) * 128].astype(BF16)
    others = [(dy, dc) for dy in range(NY) for dc in range(NC) if dy or dc]

    def sp_peer(dy, dc):
        py, pc = step(y, dy, NY), lax.rem(c + dc, NC)
        return py, pc, py * NC + pc

    sp_sum = []
    for n, (dy, dc) in enumerate(others):
        py, pc, number = sp_peer(dy, dc)
        sp_sum.append(remote(sums.at[number], sum_in.at[n], y=py, c=pc))

    for copy in z_dq_all:
        copy.wait_recv()
    for copy in c_wq:
        copy.wait_recv()
    out = jnp.zeros((32, NX * 64), F32)
    for zz in range(NZ):
        cols = slice(zz * HEAD_DIM, (zz + 1) * HEAD_DIM)
        out += mm(dq_all[zz], wq[:, :, :, cols].reshape(NX * 64, HEAD_DIM), NT)
    for half in range(2):
        dtp[half] = out[:, half * 128 : (half + 1) * 128].astype(BF16)
    x_dt = [
        remote(dtp.at[step(x, d, NX) // 2], dt_in.at[x], x=step(x, d, NX)) for d in range(1, NX)
    ]
    dt_in[x] = dtp[x // 2]

    for copy in sp_sum:
        copy.wait_recv()
    own_sum = sums[y * NC + c].astype(F32)
    for n in range(len(others)):
        own_sum += sum_in[n].astype(F32)
    total[...] = own_sum
    sp_all = []
    for dy, dc in others:
        py, pc, number = sp_peer(dy, dc)
        sp_all.append(remote(total, totals.at[y * NC + c], y=py, c=pc))
    totals[y * NC + c] = own_sum

    for copy in x_ds:
        copy.wait_recv()
    for xx in range(NX):
        rows = jnp.transpose(dst_in[xx].astype(F32)).astype(BF16)
        ds_ref[:, xx] = rows.reshape(NZ, 32, 64)
    for copy in x_dt:
        copy.wait_recv()
    odd = lax.rem(x, 2) == 1
    for xx in range(NX):
        both = dt_in[xx]
        dt_ref[xx * 32 : (xx + 1) * 32] = jnp.where(odd, both[:, 64:], both[:, :64])
    for copy in sp_all:
        copy.wait_recv()
    for j in range(16):
        dw_ref[(j // 4) * 16 : (j // 4 + 1) * 16, (j % 4) * 128 : (j % 4 + 1) * 128] = totals[j]
    for copy in made:
        copy.wait_send()


def shards(queries, attn_out, log_norm, cotangent, keys, values, source, w_query, w_key, w_value):
    lse = jnp.transpose(log_norm).reshape(KV_HEADS, 1, PER_GROUP * 128)
    kv = jnp.stack([keys, values])
    wkv = jnp.stack([w_key.reshape(2, 32, 512), w_value.reshape(2, 32, 512)], axis=1)
    vmem = pl.BlockSpec(memory_space=pltpu.VMEM)

    def bf(*shape):
        return pltpu.VMEM(shape, BF16)

    def f32(*shape):
        return pltpu.VMEM(shape, F32)

    d_target, d_source, d_wvalue = pl.pallas_call(
        kernel,
        out_shape=(
            jax.ShapeDtypeStruct((128, 64), BF16),
            jax.ShapeDtypeStruct((NZ, NX, 32, 64), BF16),
            jax.ShapeDtypeStruct((64, 512), F32),
        ),
        in_specs=[vmem] * 8,
        out_specs=(vmem,) * 3,
        scratch_shapes=[
            bf(NY, NC, 2, 32, 512),
            bf(2, 768, 256), bf(2, 768, 256), f32(2, 1, 768), f32(2, 768, 256),
            bf(NC, NY, 2, 32, 512), bf(NY, 2, 32, 512), bf(NY, 2, 32, 512),
            bf(4, 4, 32, 512), bf(4, 3, 32, 512), bf(2, 32, 512),
            bf(NX, NZ, 32, 256), bf(NX - 1, NZ, 32, 256), bf(NZ, 32, 256),
            bf(NZ - 1, 32, 256), bf(32, 256), bf(2, NZ, 32, 512), bf(NZ, 32, 256),
            bf(NX, 2, 2, 32, 512), bf(NX, 2, 32, 3072), bf(NX, NZ, 32, 64),
            bf(NX, 64, 512), bf(NX - 1, 64, 512), bf(16, 16, 128), bf(15, 16, 128),
            f32(16, 128), f32(16, 16, 128),
            bf(NX, 64, 384), bf(NX, 64, 384), bf(2, 32, 128), bf(NX, 32, 128),
            pltpu.SemaphoreType.DMA((COPIES,)), pltpu.SemaphoreType.DMA((COPIES,)),
        ],
        compiler_params=pltpu.CompilerParams(
            collective_id=0, has_side_effects=True, vmem_limit_bytes=56 * 2**20
        ),
    )(
        queries, attn_out, cotangent, lse, kv, source.reshape(NZ, NX, 32, 64), wkv,
        w_query.reshape(2, 32, 3072),
    )
    return d_target, d_source.reshape(1536, 64), d_wvalue


def solution(mesh):
    split = Mesh(mesh.devices.reshape(NY, NC, NZ, NX), ("y", "c", "z", "x"))
    sp, tp = ("y", "c"), ("z", "x")
    every = sp + tp
    in_specs = (
        P(sp, None), P(sp, None), P(sp, None), P(sp, None),
        P(every, None), P(every, None), P(sp, tp),
        P(tp, None), P(tp, None), P(tp, None),
    )
    out_specs = (P(sp, tp), P(sp, tp), P(tp, None))
    return jax.shard_map(
        shards, mesh=split, in_specs=in_specs, out_specs=out_specs, check_vma=False
    )
```

time: 259 us -> 107 us (0.41)
  blocking collectives: 134 us -> 0 us
  Pallas kernels: 0 us -> 97.9 us
  waiting for transfers between devices: 63.9 us -> 0 us
  starting transfers between devices: 19.7 us -> 0 us
  between operations: 14.2 us -> 0.65 us
  matrix products: 12.3 us -> 0 us
  local copies, waits for them, and re-layouts: 11.4 us -> 6.19 us
    pallas_call x0 -> x1, Pallas kernels: none -> 97.9 us  [shards(): pl.pallas_call(kernel, out_shape=(jax.ShapeDtypeStruct((128, 64), BF16),...]
    all_to_all x2 -> x0, blocking collectives: 78.6 us -> none  [sum_at_owner(): lax.all_to_all(parts, axis, split_axis=0, concat_axis=0, tiled=True)]
    all_gather x3 -> x0, blocking collectives: 55.8 us -> none  [the longest x1 26.4 us: shards(): lax.all_gather(keys, 'sp', axis=0, tiled=True)]
    all_gather x1 -> x0, waiting for transfers between devices: 40.3 us -> none  [whole_of(): out = lax.all_gather(out, axes[number], axis=dim, tiled=True)]
    all_to_all x2 -> x0, waiting for transfers between devices: 23.5 us -> none  [from_everyone(): lax.all_to_all(jnp.broadcast_to(array[None], (size, *array.shape)), axis,...]
    all_to_all x2 -> x0, starting transfers between devices: 19.7 us -> none  [from_everyone(): lax.all_to_all(jnp.broadcast_to(array[None], (size, *array.shape)), axis,...]
    dot_general x8 -> x0, matrix products: 12.3 us -> none  [the longest x1 2.67 us: shards(): lax.dot_general(source, group[:, kv_width:], (((0,), (0,)), ((), ())), pr...]
    broadcast_in_dim x2 -> x0, local copies, waits for them, and re-layouts: 2.98 us -> none  [from_everyone(): jnp.broadcast_to(array[None], (size, *array.shape))]
  transfers between devices with their start and end apart: 3 -> 0, of which waited for: 2 -> 0; matrix products, arithmetic and copies ran while one was open for 4% -> 0% of each run, Pallas kernels for 0% -> 0%
where the time goes in v1:
time: 107 us
  Pallas kernels  97.9 us (91%)
  local copies, waits for them, and re-layouts  6.19 us (6%)
  other arithmetic  2.12 us (2%)
    pallas_call x1, Pallas kernels, shards(): pl.pallas_call(kernel, out_shape=(jax.ShapeDtypeStruct((128, 64), BF16),...  97.9 us
    unnamed x14, local copies, waits for them, and re-layouts  5.59 us

profile of v1, /device:TPU:1, one launch (start us, length us, event | category | flops | bytes accessed | tf_op | source)
XLA Modules:
  0.0 106.8 jit_solution(17255828795676366555)
XLA Ops:
  0.6 0.0 copy-start.4
  0.6 0.7 copy-done.4
  1.3 0.0 copy-start.2
  1.3 0.0 copy-start.3
  1.3 0.6 reshape.18.lse_ref
  1.9 0.0 copy-start
  1.9 1.4 %pad_maximum_fusion.1.kv_ref = bf16[2,32,512]{2,1,0:T(8,128)(2,1)} fusion(bf16[1,32,512]{2,1,0:T(8,128)(2,1)} %bitcast.13, bf16[1,32,512]{2,1,0:T(8,128)(2,1)} %bitcast.14), kind=kLoop, calls=%fused_computation.1 | loop fusion | flops 32768 | bytes 131072 | tf_op jit(solution)/shard_map/stack | solution.py:295
  3.4 0.0 copy-done.2
  3.4 0.0 copy-done.3
  3.4 0.7 pad_maximum_fusion.wkv_ref
  4.1 0.0 copy-done
  4.1 0.9 copy.13
  5.0 97.9 %shard_map.121 = (bf16[128,64]{1,0:T(8,128)(2,1)}, bf16[12,4,32,64]{3,2,1,0:T(8,128)(2,1)}, f32[64,512]{1,0:T(8,128)}) custom-call(bf16[128,3072]{1,0:T(8,128)(2,1)} %q_ref.1, bf16[128,3072]{1,0:T(8,128)(2,1)} %o_ref.1, bf16[128,3072]{1,0:T(8,128)(2,1)} %do_ref.1, f32[2,1,768]{2,1,0:T(1,128)} %reshape.18.lse_ref, ...), custom_call_target="tpu_custom_call" | custom-call | tf_op jit(solution)/shard_map/pallas_call | solution.py:305
  102.8 1.4 %copy.14 = bf16[128,64]{0,1:T(8,128)(2,1)} copy(bf16[128,64]{1,0:T(8,128)(2,1)} %get-tuple-element.9) | data formatting | bytes 32768
  104.3 0.0 copy-start.1
  104.3 1.9 %copy.15 = bf16[1536,64]{0,1:T(8,128)(2,1)} copy(bf16[1536,64]{1,0:T(8,128)(2,1)} %bitcast.9) | data formatting | bytes 393216
  106.2 0.0 copy-done.1
  106.2 0.7 copy.17
Async XLA Ops:
  0.6 0.7 copy-start.4
  1.3 2.1 %copy-start.2 = (bf16[64,512]{1,0:T(8,128)(2,1)S(1)}, bf16[64,512]{1,0:T(8,128)(2,1)}, u32[]{:S(2)}) copy-start(bf16[64,512]{1,0:T(8,128)(2,1)} %param.19) | copy-start | bytes 196612
  1.3 2.1 %copy-start.3 = (bf16[64,512]{1,0:T(8,128)(2,1)S(1)}, bf16[64,512]{1,0:T(8,128)(2,1)}, u32[]{:S(2)}) copy-start(bf16[64,512]{1,0:T(8,128)(2,1)} %param.18) | copy-start | bytes 196612
  1.9 2.1 %copy-start = (bf16[1536,64]{0,1:T(8,128)(2,1)S(1)}, bf16[1536,64]{0,1:T(8,128)(2,1)}, u32[]{:S(2)}) copy-start(bf16[1536,64]{0,1:T(8,128)(2,1)} %param.16) | copy-start | bytes 589828
  104.3 1.9 %copy-start.1 = (f32[64,512]{1,0:T(8,128)S(1)}, f32[64,512]{1,0:T(8,128)}, u32[]{:S(2)}) copy-start(f32[64,512]{1,0:T(8,128)} %get-tuple-element.17) | copy-start | bytes 393220

commit v2 on v1

v2 whole, which is shorter than its diff:
```python
import math

import jax
import jax.numpy as jnp
from jax import lax
from jax.experimental import pallas as pl
from jax.experimental.pallas import tpu as pltpu
from jax.sharding import Mesh
from jax.sharding import PartitionSpec as P

HEADS = 12
KV_HEADS = 2
HEAD_DIM = 256
PER_GROUP = HEADS // KV_HEADS
NY, NC, NZ, NX = 8, 2, 12, 4
MESH = pl.DeviceIdType.MESH
F32 = jnp.float32
BF16 = jnp.bfloat16
NT = (((1,), (1,)), ((), ()))
TN = (((0,), (0,)), ((), ()))
NN = (((1,), (0,)), ((), ()))
Y_CHAINS = ((0, 1, 4), (1, -1, 4), (1, 1, 3), (0, -1, 3))
Z_CHAINS = ((0, 1, 6), (1, -1, 6), (1, 1, 5), (0, -1, 5))
DQ_CHAINS = ((None, 1, 6), (None, -1, 5))
Y_JUMP, Z_JUMP = 2, 2
NEAR, FAR = (0, 1, -1, 2), (4, 3, -3, -2)
COPIES, SENDS = 182, 64


def mm(a, b, dims):
    return lax.dot_general(a, b, dims, preferred_element_type=F32)


def kernel(
    q_hbm, o_hbm, do_hbm, lse_hbm, k_hbm, v_hbm, src_hbm, wk_hbm, wv_hbm, wq_hbm,
    dt_ref, ds_ref, dw_ref,
    q_ref, o_ref, do_ref, lse_ref, src_ref,
    kv, qs, dos, delta, lse, dq_acc, part, from_core, paired, ring_in, ring_out, own,
    dqp, x_in, x_sum, z_in, z_out, chunk, gathered, dq_all,
    wkv, wq, sxo, sx, wvp, wv_core, wv_half, wv_in, sums, sum_in, total, totals,
    dst_part, dst_in, ds_rows, dtp, dt_in,
    z_sem, local_sem, send_sem, recv_sem,
):
    y, c, z, x = (lax.axis_index(a) for a in ("y", "c", "z", "x"))
    scale = 1.0 / math.sqrt(HEAD_DIM)
    made = []

    def step(v, d, n):
        return lax.rem(v + d + n, n)

    def remote(src, dst, **where):
        number = len(made)
        if number >= SENDS:
            made[number - SENDS].wait_send()
        copy = pltpu.make_async_remote_copy(
            src_ref=src,
            dst_ref=dst,
            send_sem=send_sem.at[number % SENDS],
            recv_sem=recv_sem.at[number],
            device_id=where,
            device_id_type=MESH,
        )
        copy.start()
        made.append(copy)
        return copy

    def spread(copies, name, axis, here, size, d, length, jump, at, t):
        if t:
            copies[name, t].wait_recv()
        if t % jump == 0:
            for far in range(min(jump, length - t), 0, -1):
                src, dst = at(t)
                copies[name, t + far] = remote(src, dst, **{axis: step(here, d * far, size)})

    here = {}

    def load(name, src, dst):
        here[name] = pltpu.make_async_copy(src, dst, local_sem.at[len(here)])
        here[name].start()

    load("v", v_hbm, kv.at[y, c, :, 1])
    load("k", k_hbm, kv.at[y, c, :, 0])
    load("wk", wk_hbm, wkv.at[x, :, 0])
    load("wv", wv_hbm, wkv.at[x, :, 1])
    load("src", src_hbm, src_ref)
    load("q", q_hbm, q_ref)
    load("do", do_hbm, do_ref)
    load("o", o_hbm, o_ref)
    load("lse", lse_hbm, lse_ref)
    load("wq", wq_hbm, wq.at[x])

    barrier = pltpu.get_barrier_semaphore()
    peers = [{"y": step(y, d, NY)} for d in (1, -1, 2, -2)] + [{"c": 1 - c}]
    peers += [{"x": step(x, d, NX)} for d in range(1, NX)]
    peers += [{"z": step(z, 1, NZ)}, {"z": step(z, -1, NZ)}]
    for peer in peers:
        pl.semaphore_signal(barrier, inc=1, device_id=peer, device_id_type=MESH)
    here["k"].wait()
    here["v"].wait()
    pl.semaphore_wait(barrier, len(peers))

    def z_tell(number, far):
        for n, d in enumerate((1, -1)):
            pl.semaphore_signal(z_sem.at[number, n], inc=1, device_id={"z": step(z, d * far, NZ)}, device_id_type=MESH)

    def z_hear(number):
        for n in range(2):
            pl.semaphore_wait(z_sem.at[number, n], 1)

    z_tell(0, 1)
    hops = {}
    ways = {}
    core_kv = {}

    def kv_spread(t):
        for r, d, length in Y_CHAINS:
            if t > length:
                continue
            block = kv.at[step(y, -d * t, NY), c, r]
            spread(ways, (r, d), "y", y, NY, d, length, Y_JUMP, lambda t: (block, block), t)
            if t:
                core_kv[4 if t == 4 else -d * t, r] = remote(block, block, c=1 - c)

    kv_spread(0)
    core_kv[0] = remote(kv.at[y, c], kv.at[y, c], c=1 - c)
    here["wk"].wait()
    here["wv"].wait()
    x_wkv = [remote(wkv.at[x, c], wkv.at[x, c], x=step(x, d, NX)) for d in range(1, NX)]
    here["src"].wait()
    for zz in range(NZ):
        rows = jnp.transpose(src_ref[:, zz * 128 : (zz + 1) * 128].astype(F32)).astype(BF16)
        for xx in range(NX):
            sxo[xx, zz] = rows[xx * 32 : (xx + 1) * 32]
    x_src = [remote(sxo.at[step(x, d, NX)], sx.at[x], x=step(x, d, NX)) for d in range(1, NX)]

    for name in ("q", "do", "o", "lse"):
        here[name].wait()

    def prepare(g):
        for h in range(PER_GROUP):
            head = g * PER_GROUP + h
            columns = slice(head * HEAD_DIM, (head + 1) * HEAD_DIM)
            rows = slice(h * 128, (h + 1) * 128)
            qs[g, rows] = q_ref[:, columns]
            dos[g, rows] = do_ref[:, columns]
            prod = do_ref[:, columns].astype(F32) * o_ref[:, columns].astype(F32)
            halves = prod[:, :128] + prod[:, 128:]
            delta[g, :, rows] = jnp.sum(jnp.transpose(halves), axis=0, keepdims=True)
            lse[g, :, rows] = lse_ref[head : head + 1]

    def attend(offsets, first):
        for d in offsets:
            for r in range(2):
                if (d, r) in core_kv:
                    core_kv[d, r].wait_recv()
        if first:
            core_kv[0].wait_recv()
        places = [(d, lax.rem(c + dc, NC)) for d in offsets for dc in range(NC)]
        for g in range(KV_HEADS):
            cols = slice(g * HEAD_DIM, (g + 1) * HEAD_DIM)

            def rows_of(w):
                return jnp.concatenate(
                    [kv[step(y, d, NY), cc, :, w, :, cols].reshape(32, HEAD_DIM) for d, cc in places], axis=0
                )

            kb, vb = rows_of(0), rows_of(1)
            scores = mm(kb, qs[g], NT) * scale
            probs = jnp.exp(scores - lse[g])
            dprob = mm(vb, dos[g], NT)
            dscore = (probs * (dprob - delta[g])).astype(BF16)
            dk = (mm(dscore, qs[g], NN) * scale).astype(BF16)
            dv = mm(probs.astype(BF16), dos[g], NN).astype(BF16)
            term = mm(dscore, kb, TN) * scale
            at = slice(g * 768, (g + 1) * 768)
            dq_acc[at] = term if first else dq_acc[at] + term
            for n, (d, cc) in enumerate(places):
                rows = slice(n * 32, n * 32 + 32)
                part[cc, step(y, d, NY), :, 0, :, cols] = dk[rows].reshape(2, 16, HEAD_DIM)
                part[cc, step(y, d, NY), :, 1, :, cols] = dv[rows].reshape(2, 16, HEAD_DIM)

    core_in = {}

    def to_core(offsets):
        for d in offsets:
            at = step(y, d, NY)
            core_in[d] = remote(part.at[1 - c, at], from_core.at[at], c=1 - c)

    def pair(offsets):
        for d in offsets:
            core_in[d].wait_recv()
            at = step(y, d, NY)
            paired[at] = (part[c, at].astype(F32) + from_core[at].astype(F32)).astype(BF16)

    prepare(0)
    kv_spread(1)
    z_hear(0)
    z_tell(1, 2)
    prepare(1)
    kv_spread(2)
    attend(NEAR, True)
    to_core(NEAR)
    z_hear(1)
    z_tell(2, 2)
    kv_spread(3)
    kv_spread(4)
    pair(NEAR)
    attend(FAR, False)

    to_core(FAR)
    x_dq = {}
    for m in range(6):
        for s, d in enumerate((6 - m, m - 5)):
            for xx in range(NX):
                at = pl.multiple_of(step(z, d, NZ) * 128 + xx * 32, 32)
                dqp[xx, m, s] = dq_acc[pl.ds(at, 32)].astype(BF16)
        for d in range(1, NX):
            x_dq[m, d] = remote(dqp.at[step(x, d, NX), m], x_in.at[d - 1, m], x=step(x, d, NX))
    here["wq"].wait()
    x_wq = [remote(wq.at[x, c], wq.at[x, c], x=step(x, d, NX)) for d in range(1, NX)]

    pair(FAR)
    y_sent = {}

    def y_send(r, d, length, t, value_ref):
        far = 2 - t % 2
        n = Y_CHAINS.index((r, d, length))
        y_sent[r, d, t] = remote(value_ref, ring_in.at[n, t - 1], y=step(y, d * far, NY))

    for t in (4, 3):
        for r, d, length in Y_CHAINS:
            if t <= length:
                y_send(r, d, length, t, paired.at[step(y, d * t, NY), r])
    for r, d, length in Y_CHAINS:
        y_send(r, d, length, 1, paired.at[step(y, d, NY), r])

    def y_middle():
        for n, (r, d, length) in enumerate(Y_CHAINS):
            rows = paired[step(y, d * 2, NY), r].astype(F32)
            for t in range(3, length + 1):
                y_sent[r, d, t].wait_recv()
                rows += ring_in[n, t - 1].astype(F32)
            ring_out[n] = rows.astype(BF16)
            y_send(r, d, length, 2, ring_out.at[n])

    z_dq = []

    def dq_part(m):
        for d in range(1, NX):
            x_dq[m, d].wait_recv()
        rows = dqp[x, m].astype(F32)
        for d in range(1, NX):
            rows += x_in[d - 1, m].astype(F32)
        for s, d in enumerate((6 - m, m - 5)):
            if d:
                z_out[s, m] = rows[s].astype(BF16)
                z_dq.append((s, m, remote(z_out.at[s, m], z_in.at[s, m], z=step(z, d, NZ))))
            else:
                x_sum[...] = rows[s]

    z_hear(2)
    dq_part(0)
    y_middle()
    for m in range(1, 4):
        dq_part(m)
    for r in range(2):
        rows = paired[y, r].astype(F32)
        for n, (r_, d, length) in enumerate(Y_CHAINS):
            if r_ == r:
                for t in (1, 2):
                    y_sent[r, d, t].wait_recv()
                    rows += ring_in[n, t - 1].astype(F32)
        for w in range(2):
            own[w, r] = rows[w].astype(BF16)

    def over_z(w, t):
        for r, d, length in Z_CHAINS:
            if t > length:
                continue
            at = step(z, -d * t, NZ)
            block = gathered.at[w, at, r]
            src = block if t else own.at[w, r]
            spread(ways, (w, r, d), "z", z, NZ, d, length, Z_JUMP, lambda t: (src, block), t)

    def dq_over_z(t):
        for _, d, length in DQ_CHAINS:
            if t > length:
                continue
            block = dq_all.at[step(z, -d * t, NZ)]
            src = block if t else chunk
            spread(ways, ("dq", d), "z", z, NZ, d, length, Z_JUMP, lambda t: (src, block), t)

    over_z(1, 0)
    for w in range(2):
        gathered[w, z] = own[w]
    dq_part(4)
    dq_part(5)
    for d in range(1, NX):
        x_wkv[d - 1].wait_recv()
    c_wkv = [remote(wkv.at[step(x, -d, NX), c], wkv.at[step(x, -d, NX), c], c=1 - c) for d in range(1, NX)]
    for copy in x_src:
        copy.wait_recv()
    sx[x] = sxo[x]
    over_z(1, 1)
    over_z(1, 2)
    over_z(0, 0)
    dq_rows = x_sum[...]
    for s, m, copy in z_dq:
        copy.wait_recv()
        dq_rows += z_in[s, m].astype(F32)
    chunk[...] = dq_rows.astype(BF16)
    dq_over_z(0)
    dq_all[z] = chunk[...]
    over_z(1, 3)
    over_z(1, 4)
    over_z(0, 1)
    over_z(0, 2)
    dq_over_z(1)
    dq_over_z(2)
    over_z(1, 5)
    over_z(1, 6)

    dv_rows = gathered[1].reshape(NZ * 32, 512)
    for xx in range(NX):
        term = mm(sx[xx].reshape(NZ * 32, 64), dv_rows, TN).astype(BF16)
        for half in range(2):
            wvp[half, xx] = term[:, half * 256 : (half + 1) * 256]
    core_wv = remote(wvp.at[1 - c], wv_core, c=1 - c)
    over_z(0, 3)
    over_z(0, 4)
    core_wv.wait_recv()
    wv_half[...] = (wvp[c].astype(F32) + wv_core[...].astype(F32)).astype(BF16)
    x_wv = [remote(wv_half.at[step(x, d, NX)], wv_in.at[d - 1], x=step(x, d, NX)) for d in range(1, NX)]
    dq_over_z(3)
    dq_over_z(4)
    for d in range(1, NX):
        x_wq[d - 1].wait_recv()
    c_wq = [remote(wq.at[step(x, -d, NX), c], wq.at[step(x, -d, NX), c], c=1 - c) for d in range(1, NX)]
    for copy in x_wv:
        copy.wait_recv()
    w_sum = wv_half[x].astype(F32)
    for d in range(1, NX):
        w_sum += wv_in[d - 1].astype(F32)
    for j in range(NY):
        sums[j] = w_sum[(j // 2) * 16 : (j // 2 + 1) * 16, (j % 2) * 128 : (j % 2 + 1) * 128].astype(BF16)
    y_sum = [remote(sums.at[step(y, d, NY)], sum_in.at[d - 1], y=step(y, d, NY)) for d in range(1, NY)]
    over_z(0, 5)
    over_z(0, 6)
    for copy in c_wkv:
        copy.wait_recv()
    dk_rows = gathered[0].reshape(NZ * 32, 512)
    w_key = wkv[:, :, 0].reshape(NX * 64, 512)
    w_value = wkv[:, :, 1].reshape(NX * 64, 512)
    grad = mm(w_key, dk_rows, NT) + mm(w_value, dv_rows, NT)
    for xx in range(NX):
        dst_part[xx] = grad[xx * 64 : (xx + 1) * 64].astype(BF16)
    x_ds = [remote(dst_part.at[step(x, d, NX)], dst_in.at[x], x=step(x, d, NX)) for d in range(1, NX)]
    dst_in[x] = dst_part[x]
    dq_over_z(5)
    dq_over_z(6)
    for copy in c_wq:
        copy.wait_recv()
    out = jnp.zeros((32, NX * 64), F32)
    for zz in range(NZ):
        cols = slice(zz * HEAD_DIM, (zz + 1) * HEAD_DIM)
        out += mm(dq_all[zz], wq[:, :, :, cols].reshape(NX * 64, HEAD_DIM), NT)
    for half in range(2):
        dtp[half] = out[:, half * 128 : (half + 1) * 128].astype(BF16)
    x_dt = [remote(dtp.at[step(x, d, NX) // 2], dt_in.at[x], x=step(x, d, NX)) for d in range(1, NX)]
    dt_in[x] = dtp[x // 2]
    for copy in y_sum:
        copy.wait_recv()
    own_sum = sums[y].astype(F32)
    for d in range(1, NY):
        own_sum += sum_in[d - 1].astype(F32)
    total[...] = own_sum.astype(BF16)
    sp_all = [
        remote(total, totals.at[y, c], y=step(y, dy, NY), c=lax.rem(c + dc, NC))
        for dy in range(NY)
        for dc in range(NC)
        if dy or dc
    ]
    totals[y, c] = own_sum.astype(BF16)

    for copy in x_ds:
        copy.wait_recv()
    for xx in range(NX):
        ds_rows[:, xx] = jnp.transpose(dst_in[xx].astype(F32)).reshape(NZ, 32, 64)
    for zz in range(NZ):
        ds_ref[:, zz * 128 : (zz + 1) * 128] = jnp.transpose(ds_rows[zz].reshape(128, 64)).astype(BF16)
    for copy in x_dt:
        copy.wait_recv()
    both = jnp.transpose(dt_in[...].reshape(128, 128).astype(F32))
    dt_ref[...] = jnp.where(lax.rem(x, 2) == 1, both[64:], both[:64]).astype(BF16)
    for copy in sp_all:
        copy.wait_recv()
    for j in range(NY):
        for cc in range(NC):
            lanes = slice(cc * 256 + (j % 2) * 128, cc * 256 + (j % 2 + 1) * 128)
            dw_ref[(j // 2) * 16 : (j // 2 + 1) * 16, lanes] = totals[j, cc].astype(F32)
    for copy in made[-SENDS:]:
        copy.wait_send()


def put(dt_ref, ds_ref, dw_ref, dt_out, ds_out, dw_out, sem):
    copies = [
        pltpu.make_async_copy(src, dst, sem.at[n])
        for n, (src, dst) in enumerate(((dt_ref, dt_out), (ds_ref, ds_out), (dw_ref, dw_out)))
    ]
    for copy in copies:
        copy.start()
    for copy in copies:
        copy.wait()


def shards(queries, attn_out, log_norm, cotangent, keys, values, source, w_query, w_key, w_value):
    hbm = pl.BlockSpec(memory_space=pl.ANY)
    vmem = pl.BlockSpec(memory_space=pltpu.VMEM)

    def bf(*shape):
        return pltpu.VMEM(shape, BF16)

    def f32(*shape):
        return pltpu.VMEM(shape, F32)

    d_target, d_source, d_wvalue = pl.pallas_call(
        kernel,
        out_shape=(bf(64, 128), bf(64, 1536), f32(64, 512)),
        in_specs=[hbm] * 10,
        out_specs=(vmem,) * 3,
        scratch_shapes=[
            bf(128, 3072), bf(128, 3072), bf(128, 3072), f32(12, 128), bf(64, 1536),
            bf(NY, NC, 2, 2, 16, 512),
            bf(2, 768, 256), bf(2, 768, 256), f32(2, 1, 768), f32(2, 1, 768), f32(1536, 256),
            bf(NC, NY, 2, 2, 16, 512), bf(NY, 2, 2, 16, 512), bf(NY, 2, 2, 16, 512),
            bf(4, 4, 2, 16, 512), bf(4, 2, 16, 512), bf(2, 2, 16, 512),
            bf(NX, 6, 2, 32, 256), bf(NX - 1, 6, 2, 32, 256), f32(32, 256),
            bf(2, 6, 32, 256), bf(2, 6, 32, 256), bf(32, 256),
            bf(2, NZ, 2, 16, 512), bf(NZ, 32, 256),
            bf(NX, 2, 2, 32, 512), bf(NX, 2, 32, 3072), bf(NX, NZ, 32, 64), bf(NX, NZ, 32, 64),
            bf(2, NX, 64, 256), bf(NX, 64, 256), bf(NX, 64, 256), bf(NX - 1, 64, 256),
            bf(NY, 16, 128), bf(NY - 1, 16, 128), bf(16, 128), bf(NY, NC, 16, 128),
            bf(NX, 64, 384), bf(NX, 64, 384), f32(NZ, NX, 32, 64), bf(2, 32, 128), bf(NX, 32, 128),
            pltpu.SemaphoreType.REGULAR((3, 2)), pltpu.SemaphoreType.DMA((10,)),
            pltpu.SemaphoreType.DMA((SENDS,)), pltpu.SemaphoreType.DMA((COPIES,)),
        ],
        compiler_params=pltpu.CompilerParams(
            collective_id=0, has_side_effects=True, vmem_limit_bytes=56 * 2**20
        ),
    )(
        queries, attn_out, cotangent, jnp.transpose(log_norm),
        keys.reshape(2, 16, 512), values.reshape(2, 16, 512), jnp.transpose(source),
        w_key.reshape(2, 32, 512), w_value.reshape(2, 32, 512), w_query.reshape(2, 32, 3072),
    )
    d_target, d_source, d_wvalue = pl.pallas_call(
        put,
        out_shape=(
            jax.ShapeDtypeStruct((64, 128), BF16),
            jax.ShapeDtypeStruct((64, 1536), BF16),
            jax.ShapeDtypeStruct((64, 512), F32),
        ),
        in_specs=[vmem] * 3,
        out_specs=(hbm,) * 3,
        scratch_shapes=[pltpu.SemaphoreType.DMA((3,))],
    )(*(pltpu.with_memory_space_constraint(a, pltpu.VMEM) for a in (d_target, d_source, d_wvalue)))
    return jnp.transpose(d_target), jnp.transpose(d_source), d_wvalue


def solution(mesh):
    split = Mesh(mesh.devices.reshape(NY, NC, NZ, NX), ("y", "c", "z", "x"))
    sp, tp = ("y", "c"), ("z", "x")
    every = sp + tp
    in_specs = (
        P(sp, None), P(sp, None), P(sp, None), P(sp, None),
        P(every, None), P(every, None), P(sp, tp),
        P(tp, None), P(tp, None), P(tp, None),
    )
    out_specs = (P(sp, tp), P(sp, tp), P(tp, None))
    return jax.shard_map(
        shards, mesh=split, in_specs=in_specs, out_specs=out_specs, check_vma=False
    )
```

time: 107 us -> 76.2 us (0.71)
  Pallas kernels: 97.9 us -> 75.4 us
  local copies, waits for them, and re-layouts: 6.19 us -> 0 us
  other arithmetic: 2.12 us -> 0 us
    pallas_call x1 -> x2, Pallas kernels: 97.9 us -> 75.4 us  [the longest x1 74.7 us: shards(): pl.pallas_call(kernel, out_shape=(bf(64, 128), bf(64, 1536), f32(64, 512)...]
    unnamed x14 -> x0, local copies, waits for them, and re-layouts: 5.59 us -> none
    another operation x2 -> x0, other arithmetic: 2.12 us -> none  [the longest x1 1.45 us: shards(): kv = jnp.stack([keys, values])]
where the time goes in v2:
time: 76.2 us; the launch traced here: 76.1 us
  Pallas kernels  75.4 us (99%)
    pallas_call x1, Pallas kernels, shards(): pl.pallas_call(kernel, out_shape=(bf(64, 128), bf(64, 1536), f32(64, 512)...  74.7 us

profile of v2, /device:TPU:1, one launch (start us, length us, event | category | flops | bytes accessed | tf_op | source)
XLA Modules:
  0.0 76.1 jit_solution(6375674897576605777)
XLA Ops:
  0.6 74.7 %shard_map.121 = (bf16[64,128]{1,0:T(8,128)(2,1)S(1)}, bf16[64,1536]{1,0:T(8,128)(2,1)S(1)}, f32[64,512]{1,0:T(8,128)S(1)}) custom-call(bf16[128,3072]{1,0:T(8,128)(2,1)} %q_hbm.1, bf16[128,3072]{1,0:T(8,128)(2,1)} %o_hbm.1, bf16[128,3072]{1,0:T(8,128)(2,1)} %do_hbm.1, f32[12,128]{1,0:T(8,128)} %bitcast.15, bf16[2,16,512]{2,1,0:T(8,128)(2,1)} %bitcast.13, ...), custom_call_target="tpu_custom_call" | custom-call | tf_op jit(solution)/shard_map/pallas_call | solution.py:426
  75.3 0.8 shard_map.122

commit v3 on v2

--- a/solution.py
+++ b/solution.py
@@ -24,7 +24,7 @@
 DQ_CHAINS = ((None, 1, 6), (None, -1, 5))
 Y_JUMP, Z_JUMP = 2, 2
 NEAR, FAR = (0, 1, -1, 2), (4, 3, -3, -2)
-COPIES, SENDS = 182, 64
+COPIES, SENDS = 196, 64
 
 
 def mm(a, b, dims):
@@ -78,6 +78,19 @@
         here[name] = pltpu.make_async_copy(src, dst, local_sem.at[len(here)])
         here[name].start()
 
+    barrier = pltpu.get_barrier_semaphore()
+    peers = [{"y": step(y, d, NY)} for d in (1, -1, 2, -2)] + [{"c": 1 - c}]
+    peers += [{"x": step(x, d, NX)} for d in range(1, NX)]
+    for peer in peers:
+        pl.semaphore_signal(barrier, inc=1, device_id=peer, device_id_type=MESH)
+    near_z = [step(z, d, NZ) for d in (1, -1, 2, -2)]
+    lower = (z + 1) // NZ + (z - 1 + NZ) // NZ + (z + 2) // NZ + (z - 2 + NZ) // NZ
+
+    def greet(sem, to):
+        pl.semaphore_signal(sem, inc=1, device_id={"z": to}, device_id_type=MESH)
+
+    for to in near_z:
+        pl.when(to > z)(lambda to=to: greet(barrier, to))
     load("v", v_hbm, kv.at[y, c, :, 1])
     load("k", k_hbm, kv.at[y, c, :, 0])
     load("wk", wk_hbm, wkv.at[x, :, 0])
@@ -89,25 +102,12 @@
     load("lse", lse_hbm, lse_ref)
     load("wq", wq_hbm, wq.at[x])
 
-    barrier = pltpu.get_barrier_semaphore()
-    peers = [{"y": step(y, d, NY)} for d in (1, -1, 2, -2)] + [{"c": 1 - c}]
-    peers += [{"x": step(x, d, NX)} for d in range(1, NX)]
-    peers += [{"z": step(z, 1, NZ)}, {"z": step(z, -1, NZ)}]
-    for peer in peers:
-        pl.semaphore_signal(barrier, inc=1, device_id=peer, device_id_type=MESH)
     here["k"].wait()
     here["v"].wait()
-    pl.semaphore_wait(barrier, len(peers))
-
-    def z_tell(number, far):
-        for n, d in enumerate((1, -1)):
-            pl.semaphore_signal(z_sem.at[number, n], inc=1, device_id={"z": step(z, d * far, NZ)}, device_id_type=MESH)
-
-    def z_hear(number):
-        for n in range(2):
-            pl.semaphore_wait(z_sem.at[number, n], 1)
-
-    z_tell(0, 1)
+    pl.semaphore_wait(barrier, len(peers) + lower)
+    for to in near_z:
+        pl.when(to < z)(lambda to=to: greet(z_sem, to))
+
     hops = {}
     ways = {}
     core_kv = {}
@@ -194,14 +194,10 @@
 
     prepare(0)
     kv_spread(1)
-    z_hear(0)
-    z_tell(1, 2)
     prepare(1)
     kv_spread(2)
     attend(NEAR, True)
     to_core(NEAR)
-    z_hear(1)
-    z_tell(2, 2)
     kv_spread(3)
     kv_spread(4)
     pair(NEAR)
@@ -222,28 +218,45 @@
     pair(FAR)
     y_sent = {}
 
-    def y_send(r, d, length, t, value_ref):
+    def y_send(w, n, t, value_ref):
         far = 2 - t % 2
-        n = Y_CHAINS.index((r, d, length))
-        y_sent[r, d, t] = remote(value_ref, ring_in.at[n, t - 1], y=step(y, d * far, NY))
-
-    for t in (4, 3):
-        for r, d, length in Y_CHAINS:
-            if t <= length:
-                y_send(r, d, length, t, paired.at[step(y, d * t, NY), r])
-    for r, d, length in Y_CHAINS:
-        y_send(r, d, length, 1, paired.at[step(y, d, NY), r])
-
-    def y_middle():
+        y_sent[w, n, t] = remote(value_ref, ring_in.at[w, n, t - 1], y=step(y, Y_CHAINS[n][1] * far, NY))
+
+    def y_start(w, distances):
+        for t in distances:
+            for n, (r, d, length) in enumerate(Y_CHAINS):
+                if t <= length:
+                    y_send(w, n, t, paired.at[step(y, d * t, NY), r, w])
+
+    for w, distances in ((1, (4, 3)), (0, (4, 3)), (1, (1,)), (0, (1,))):
+        y_start(w, distances)
+
+    def y_middle(w):
         for n, (r, d, length) in enumerate(Y_CHAINS):
-            rows = paired[step(y, d * 2, NY), r].astype(F32)
+            rows = paired[step(y, d * 2, NY), r, w].astype(F32)
             for t in range(3, length + 1):
-                y_sent[r, d, t].wait_recv()
-                rows += ring_in[n, t - 1].astype(F32)
-            ring_out[n] = rows.astype(BF16)
-            y_send(r, d, length, 2, ring_out.at[n])
-
-    z_dq = []
+                y_sent[w, n, t].wait_recv()
+                rows += ring_in[w, n, t - 1].astype(F32)
+            ring_out[w, n] = rows.astype(BF16)
+            y_send(w, n, 2, ring_out.at[w, n])
+
+    def y_end(w):
+        for r in range(2):
+            rows = paired[y, r, w].astype(F32)
+            for n, (r_, d, length) in enumerate(Y_CHAINS):
+                if r_ == r:
+                    for t in (1, 2):
+                        y_sent[w, n, t].wait_recv()
+                        rows += ring_in[w, n, t - 1].astype(F32)
+            own[w, r] = rows.astype(BF16)
+        gathered[w, z] = own[w]
+
+    z_sent = {}
+
+    def z_send(d, t, rows):
+        s = (1, -1).index(d)
+        z_out[s, t - 1] = rows.astype(BF16)
+        z_sent[d, t] = remote(z_out.at[s, t - 1], z_in.at[s, t - 1], z=step(z, d * (2 - t % 2), NZ))
 
     def dq_part(m):
         for d in range(1, NX):
@@ -251,27 +264,35 @@
         rows = dqp[x, m].astype(F32)
         for d in range(1, NX):
             rows += x_in[d - 1, m].astype(F32)
-        for s, d in enumerate((6 - m, m - 5)):
-            if d:
-                z_out[s, m] = rows[s].astype(BF16)
-                z_dq.append((s, m, remote(z_out.at[s, m], z_in.at[s, m], z=step(z, d, NZ))))
+        for s, offset in enumerate((6 - m, m - 5)):
+            d, t = (1, -1)[s], abs(offset)
+            if t == 6 or t % 2:
+                z_send(d, t, rows[s])
             else:
-                x_sum[...] = rows[s]
-
-    z_hear(2)
+                x_sum[s, t // 2] = rows[s]
+
+    def z_arrived(d, t):
+        z_sent[d, t].wait_recv()
+        return z_in[(1, -1).index(d), t - 1].astype(F32)
+
+    def z_middle(t):
+        for s, (d, length) in enumerate(((1, 6), (-1, 5))):
+            rows = x_sum[s, t // 2]
+            for far in (1, 2):
+                if t + far <= length:
+                    rows += z_arrived(d, t + far)
+            z_send(d, t, rows)
+
+    @pl.when(z < NZ - 1)
+    def _():
+        pl.semaphore_wait(z_sem, 4 - lower)
+
     dq_part(0)
-    y_middle()
+    y_middle(1)
+    y_middle(0)
     for m in range(1, 4):
         dq_part(m)
-    for r in range(2):
-        rows = paired[y, r].astype(F32)
-        for n, (r_, d, length) in enumerate(Y_CHAINS):
-            if r_ == r:
-                for t in (1, 2):
-                    y_sent[r, d, t].wait_recv()
-                    rows += ring_in[n, t - 1].astype(F32)
-        for w in range(2):
-            own[w, r] = rows[w].astype(BF16)
+    y_end(1)
 
     def over_z(w, t):
         for r, d, length in Z_CHAINS:
@@ -291,8 +312,8 @@
             spread(ways, ("dq", d), "z", z, NZ, d, length, Z_JUMP, lambda t: (src, block), t)
 
     over_z(1, 0)
-    for w in range(2):
-        gathered[w, z] = own[w]
+    y_end(0)
+    z_middle(4)
     dq_part(4)
     dq_part(5)
     for d in range(1, NX):
@@ -303,20 +324,19 @@
     sx[x] = sxo[x]
     over_z(1, 1)
     over_z(1, 2)
+    z_middle(2)
     over_z(0, 0)
-    dq_rows = x_sum[...]
-    for s, m, copy in z_dq:
-        copy.wait_recv()
-        dq_rows += z_in[s, m].astype(F32)
+    over_z(1, 3)
+    over_z(1, 4)
+    dq_rows = x_sum[1, 0]
+    for d in (1, -1):
+        for t in (1, 2):
+            dq_rows += z_arrived(d, t)
     chunk[...] = dq_rows.astype(BF16)
     dq_over_z(0)
     dq_all[z] = chunk[...]
-    over_z(1, 3)
-    over_z(1, 4)
     over_z(0, 1)
     over_z(0, 2)
-    dq_over_z(1)
-    dq_over_z(2)
     over_z(1, 5)
     over_z(1, 6)
 
@@ -326,11 +346,13 @@
         for half in range(2):
             wvp[half, xx] = term[:, half * 256 : (half + 1) * 256]
     core_wv = remote(wvp.at[1 - c], wv_core, c=1 - c)
-    over_z(0, 3)
-    over_z(0, 4)
+    dq_over_z(1)
+    dq_over_z(2)
     core_wv.wait_recv()
     wv_half[...] = (wvp[c].astype(F32) + wv_core[...].astype(F32)).astype(BF16)
     x_wv = [remote(wv_half.at[step(x, d, NX)], wv_in.at[d - 1], x=step(x, d, NX)) for d in range(1, NX)]
+    over_z(0, 3)
+    over_z(0, 4)
     dq_over_z(3)
     dq_over_z(4)
     for d in range(1, NX):
@@ -433,15 +455,15 @@
             bf(NY, NC, 2, 2, 16, 512),
             bf(2, 768, 256), bf(2, 768, 256), f32(2, 1, 768), f32(2, 1, 768), f32(1536, 256),
             bf(NC, NY, 2, 2, 16, 512), bf(NY, 2, 2, 16, 512), bf(NY, 2, 2, 16, 512),
-            bf(4, 4, 2, 16, 512), bf(4, 2, 16, 512), bf(2, 2, 16, 512),
-            bf(NX, 6, 2, 32, 256), bf(NX - 1, 6, 2, 32, 256), f32(32, 256),
+            bf(2, 4, 4, 16, 512), bf(2, 4, 16, 512), bf(2, 2, 16, 512),
+            bf(NX, 6, 2, 32, 256), bf(NX - 1, 6, 2, 32, 256), f32(2, 3, 32, 256),
             bf(2, 6, 32, 256), bf(2, 6, 32, 256), bf(32, 256),
             bf(2, NZ, 2, 16, 512), bf(NZ, 32, 256),
             bf(NX, 2, 2, 32, 512), bf(NX, 2, 32, 3072), bf(NX, NZ, 32, 64), bf(NX, NZ, 32, 64),
             bf(2, NX, 64, 256), bf(NX, 64, 256), bf(NX, 64, 256), bf(NX - 1, 64, 256),
             bf(NY, 16, 128), bf(NY - 1, 16, 128), bf(16, 128), bf(NY, NC, 16, 128),
             bf(NX, 64, 384), bf(NX, 64, 384), f32(NZ, NX, 32, 64), bf(2, 32, 128), bf(NX, 32, 128),
-            pltpu.SemaphoreType.REGULAR((3, 2)), pltpu.SemaphoreType.DMA((10,)),
+            pltpu.SemaphoreType.REGULAR, pltpu.SemaphoreType.DMA((10,)),
             pltpu.SemaphoreType.DMA((SENDS,)), pltpu.SemaphoreType.DMA((COPIES,)),
         ],
         compiler_params=pltpu.CompilerParams(

time: 76.2 us -> 74 us (0.971)
  Pallas kernels: 75.4 us -> 73.2 us
    pallas_call x1, Pallas kernels: 74.7 us -> 72.4 us  [shards(): pl.pallas_call(kernel, out_shape=(bf(64, 128), bf(64, 1536), f32(64, 512)...]
where the time goes in v3:
time: 74 us; the launch traced here: 73.8 us
  Pallas kernels  73.2 us (99%)
    pallas_call x1, Pallas kernels, shards(): pl.pallas_call(kernel, out_shape=(bf(64, 128), bf(64, 1536), f32(64, 512)...  72.4 us

profile of v3, /device:TPU:1, one launch (start us, length us, event | category | flops | bytes accessed | tf_op | source)
XLA Modules:
  0.0 73.8 jit_solution(9600907483143643274)
XLA Ops:
  0.6 72.4 %shard_map.121 = (bf16[64,128]{1,0:T(8,128)(2,1)S(1)}, bf16[64,1536]{1,0:T(8,128)(2,1)S(1)}, f32[64,512]{1,0:T(8,128)S(1)}) custom-call(bf16[128,3072]{1,0:T(8,128)(2,1)} %q_hbm.1, bf16[128,3072]{1,0:T(8,128)(2,1)} %o_hbm.1, bf16[128,3072]{1,0:T(8,128)(2,1)} %do_hbm.1, f32[12,128]{1,0:T(8,128)} %bitcast.15, bf16[2,16,512]{2,1,0:T(8,128)(2,1)} %bitcast.13, ...), custom_call_target="tpu_custom_call" | custom-call | tf_op jit(solution)/shard_map/pallas_call | solution.py:448
  73.1 0.8 %shard_map.122 = (bf16[64,128]{1,0:T(8,128)(2,1)}, bf16[64,1536]{1,0:T(8,128)(2,1)}, f32[64,512]{1,0:T(8,128)}) custom-call(bf16[64,128]{1,0:T(8,128)(2,1)S(1)} %get-tuple-element.9.dt_ref, bf16[64,1536]{1,0:T(8,128)(2,1)S(1)} %get-tuple-element.10.ds_ref, f32[64,512]{1,0:T(8,128)S(1)} %get-tuple-element.11.dw_ref), custom_call_target="tpu_custom_call" | custom-call | tf_op jit(solution)/shard_map/pallas_call | solution.py:477

commit v4 on v3

--- a/solution.py
+++ b/solution.py
@@ -24,7 +24,7 @@
 DQ_CHAINS = ((None, 1, 6), (None, -1, 5))
 Y_JUMP, Z_JUMP = 2, 2
 NEAR, FAR = (0, 1, -1, 2), (4, 3, -3, -2)
-COPIES, SENDS = 196, 64
+COPIES, SENDS = 158, 64
 
 
 def mm(a, b, dims):
@@ -43,20 +43,26 @@
 ):
     y, c, z, x = (lax.axis_index(a) for a in ("y", "c", "z", "x"))
     scale = 1.0 / math.sqrt(HEAD_DIM)
-    made = []
+    made, places, groups = [], [], {}
 
     def step(v, d, n):
         return lax.rem(v + d + n, n)
 
-    def remote(src, dst, **where):
+    def remote(src, dst, group=None, **where):
         number = len(made)
+        place = groups.get(group)
+        if place is None:
+            place = len(places)
+            places.append(group)
+            if group is not None:
+                groups[group] = place
         if number >= SENDS:
             made[number - SENDS].wait_send()
         copy = pltpu.make_async_remote_copy(
             src_ref=src,
             dst_ref=dst,
             send_sem=send_sem.at[number % SENDS],
-            recv_sem=recv_sem.at[number],
+            recv_sem=recv_sem.at[place],
             device_id=where,
             device_id_type=MESH,
         )
@@ -71,6 +77,9 @@
             for far in range(min(jump, length - t), 0, -1):
                 src, dst = at(t)
                 copies[name, t + far] = remote(src, dst, **{axis: step(here, d * far, size)})
+
+    def take(group, whole):
+        pltpu.make_async_copy(whole, whole, recv_sem.at[groups[group]]).wait()
 
     here = {}
 
@@ -204,14 +213,13 @@
     attend(FAR, False)
 
     to_core(FAR)
-    x_dq = {}
     for m in range(6):
         for s, d in enumerate((6 - m, m - 5)):
             for xx in range(NX):
                 at = pl.multiple_of(step(z, d, NZ) * 128 + xx * 32, 32)
                 dqp[xx, m, s] = dq_acc[pl.ds(at, 32)].astype(BF16)
         for d in range(1, NX):
-            x_dq[m, d] = remote(dqp.at[step(x, d, NX), m], x_in.at[d - 1, m], x=step(x, d, NX))
+            remote(dqp.at[step(x, d, NX), m], x_in.at[m, d - 1], ("x_dq", m), x=step(x, d, NX))
     here["wq"].wait()
     x_wq = [remote(wq.at[x, c], wq.at[x, c], x=step(x, d, NX)) for d in range(1, NX)]
 
@@ -259,11 +267,10 @@
         z_sent[d, t] = remote(z_out.at[s, t - 1], z_in.at[s, t - 1], z=step(z, d * (2 - t % 2), NZ))
 
     def dq_part(m):
-        for d in range(1, NX):
-            x_dq[m, d].wait_recv()
+        take(("x_dq", m), x_in.at[m])
         rows = dqp[x, m].astype(F32)
         for d in range(1, NX):
-            rows += x_in[d - 1, m].astype(F32)
+            rows += x_in[m, d - 1].astype(F32)
         for s, offset in enumerate((6 - m, m - 5)):
             d, t = (1, -1)[s], abs(offset)
             if t == 6 or t % 2:
@@ -350,7 +357,7 @@
     dq_over_z(2)
     core_wv.wait_recv()
     wv_half[...] = (wvp[c].astype(F32) + wv_core[...].astype(F32)).astype(BF16)
-    x_wv = [remote(wv_half.at[step(x, d, NX)], wv_in.at[d - 1], x=step(x, d, NX)) for d in range(1, NX)]
+    [remote(wv_half.at[step(x, d, NX)], wv_in.at[d - 1], "x_wv", x=step(x, d, NX)) for d in range(1, NX)]
     over_z(0, 3)
     over_z(0, 4)
     dq_over_z(3)
@@ -358,14 +365,13 @@
     for d in range(1, NX):
         x_wq[d - 1].wait_recv()
     c_wq = [remote(wq.at[step(x, -d, NX), c], wq.at[step(x, -d, NX), c], c=1 - c) for d in range(1, NX)]
-    for copy in x_wv:
-        copy.wait_recv()
+    take("x_wv", wv_in)
     w_sum = wv_half[x].astype(F32)
     for d in range(1, NX):
         w_sum += wv_in[d - 1].astype(F32)
     for j in range(NY):
         sums[j] = w_sum[(j // 2) * 16 : (j // 2 + 1) * 16, (j % 2) * 128 : (j % 2 + 1) * 128].astype(BF16)
-    y_sum = [remote(sums.at[step(y, d, NY)], sum_in.at[d - 1], y=step(y, d, NY)) for d in range(1, NY)]
+    [remote(sums.at[step(y, d, NY)], sum_in.at[d - 1], "y_sum", y=step(y, d, NY)) for d in range(1, NY)]
     over_z(0, 5)
     over_z(0, 6)
     for copy in c_wkv:
@@ -376,7 +382,7 @@
     grad = mm(w_key, dk_rows, NT) + mm(w_value, dv_rows, NT)
     for xx in range(NX):
         dst_part[xx] = grad[xx * 64 : (xx + 1) * 64].astype(BF16)
-    x_ds = [remote(dst_part.at[step(x, d, NX)], dst_in.at[x], x=step(x, d, NX)) for d in range(1, NX)]
+    [remote(dst_part.at[step(x, d, NX)], dst_in.at[x], "x_ds", x=step(x, d, NX)) for d in range(1, NX)]
     dst_in[x] = dst_part[x]
     dq_over_z(5)
     dq_over_z(6)
@@ -388,38 +394,34 @@
         out += mm(dq_all[zz], wq[:, :, :, cols].reshape(NX * 64, HEAD_DIM), NT)
     for half in range(2):
         dtp[half] = out[:, half * 128 : (half + 1) * 128].astype(BF16)
-    x_dt = [remote(dtp.at[step(x, d, NX) // 2], dt_in.at[x], x=step(x, d, NX)) for d in range(1, NX)]
+    [remote(dtp.at[step(x, d, NX) // 2], dt_in.at[x], "x_dt", x=step(x, d, NX)) for d in range(1, NX)]
     dt_in[x] = dtp[x // 2]
-    for copy in y_sum:
-        copy.wait_recv()
+    take("y_sum", sum_in)
     own_sum = sums[y].astype(F32)
     for d in range(1, NY):
         own_sum += sum_in[d - 1].astype(F32)
     total[...] = own_sum.astype(BF16)
-    sp_all = [
-        remote(total, totals.at[y, c], y=step(y, dy, NY), c=lax.rem(c + dc, NC))
+    [
+        remote(total, totals.at[y * NC + c], "sp_all", y=step(y, dy, NY), c=lax.rem(c + dc, NC))
         for dy in range(NY)
         for dc in range(NC)
         if dy or dc
     ]
-    totals[y, c] = own_sum.astype(BF16)
-
-    for copy in x_ds:
-        copy.wait_recv()
+    totals[y * NC + c] = own_sum.astype(BF16)
+
+    take("x_ds", dst_in.at[pl.ds(0, NX - 1)])
     for xx in range(NX):
         ds_rows[:, xx] = jnp.transpose(dst_in[xx].astype(F32)).reshape(NZ, 32, 64)
     for zz in range(NZ):
         ds_ref[:, zz * 128 : (zz + 1) * 128] = jnp.transpose(ds_rows[zz].reshape(128, 64)).astype(BF16)
-    for copy in x_dt:
-        copy.wait_recv()
+    take("x_dt", dt_in.at[pl.ds(0, NX - 1)])
     both = jnp.transpose(dt_in[...].reshape(128, 128).astype(F32))
     dt_ref[...] = jnp.where(lax.rem(x, 2) == 1, both[64:], both[:64]).astype(BF16)
-    for copy in sp_all:
-        copy.wait_recv()
+    take("sp_all", totals.at[pl.ds(0, NY * NC - 1)])
     for j in range(NY):
         for cc in range(NC):
             lanes = slice(cc * 256 + (j % 2) * 128, cc * 256 + (j % 2 + 1) * 128)
-            dw_ref[(j // 2) * 16 : (j // 2 + 1) * 16, lanes] = totals[j, cc].astype(F32)
+            dw_ref[(j // 2) * 16 : (j // 2 + 1) * 16, lanes] = totals[j * NC + cc].astype(F32)
     for copy in made[-SENDS:]:
         copy.wait_send()
 
@@ -456,12 +458,12 @@
             bf(2, 768, 256), bf(2, 768, 256), f32(2, 1, 768), f32(2, 1, 768), f32(1536, 256),
             bf(NC, NY, 2, 2, 16, 512), bf(NY, 2, 2, 16, 512), bf(NY, 2, 2, 16, 512),
             bf(2, 4, 4, 16, 512), bf(2, 4, 16, 512), bf(2, 2, 16, 512),
-            bf(NX, 6, 2, 32, 256), bf(NX - 1, 6, 2, 32, 256), f32(2, 3, 32, 256),
+            bf(NX, 6, 2, 32, 256), bf(6, NX - 1, 2, 32, 256), f32(2, 3, 32, 256),
             bf(2, 6, 32, 256), bf(2, 6, 32, 256), bf(32, 256),
             bf(2, NZ, 2, 16, 512), bf(NZ, 32, 256),
             bf(NX, 2, 2, 32, 512), bf(NX, 2, 32, 3072), bf(NX, NZ, 32, 64), bf(NX, NZ, 32, 64),
             bf(2, NX, 64, 256), bf(NX, 64, 256), bf(NX, 64, 256), bf(NX - 1, 64, 256),
-            bf(NY, 16, 128), bf(NY - 1, 16, 128), bf(16, 128), bf(NY, NC, 16, 128),
+            bf(NY, 16, 128), bf(NY - 1, 16, 128), bf(16, 128), bf(NY * NC, 16, 128),
             bf(NX, 64, 384), bf(NX, 64, 384), f32(NZ, NX, 32, 64), bf(2, 32, 128), bf(NX, 32, 128),
             pltpu.SemaphoreType.REGULAR, pltpu.SemaphoreType.DMA((10,)),
             pltpu.SemaphoreType.DMA((SENDS,)), pltpu.SemaphoreType.DMA((COPIES,)),

time: 74 us -> 73.6 us (level)
  no operation moved by 1% of the time
where the time goes in v4:
time: 73.6 us; the launch traced here: 73.5 us
  Pallas kernels  72.8 us (99%)
    pallas_call x1, Pallas kernels, shards(): pl.pallas_call(kernel, out_shape=(bf(64, 128), bf(64, 1536), f32(64, 512)...  72.1 us

profile of v4, /device:TPU:1, one launch (start us, length us, event | category | flops | bytes accessed | tf_op | source)
XLA Modules:
  0.0 73.5 jit_solution(11418377676699428019)
XLA Ops:
  0.6 72.1 %shard_map.121 = (bf16[64,128]{1,0:T(8,128)(2,1)S(1)}, bf16[64,1536]{1,0:T(8,128)(2,1)S(1)}, f32[64,512]{1,0:T(8,128)S(1)}) custom-call(bf16[128,3072]{1,0:T(8,128)(2,1)} %q_hbm.1, bf16[128,3072]{1,0:T(8,128)(2,1)} %o_hbm.1, bf16[128,3072]{1,0:T(8,128)(2,1)} %do_hbm.1, f32[12,128]{1,0:T(8,128)} %bitcast.15, bf16[2,16,512]{2,1,0:T(8,128)(2,1)} %bitcast.13, ...), custom_call_target="tpu_custom_call" | custom-call | tf_op jit(solution)/shard_map/pallas_call | solution.py:450
  72.7 0.8 %shard_map.122 = (bf16[64,128]{1,0:T(8,128)(2,1)}, bf16[64,1536]{1,0:T(8,128)(2,1)}, f32[64,512]{1,0:T(8,128)}) custom-call(bf16[64,128]{1,0:T(8,128)(2,1)S(1)} %get-tuple-element.9.dt_ref, bf16[64,1536]{1,0:T(8,128)(2,1)S(1)} %get-tuple-element.10.ds_ref, f32[64,512]{1,0:T(8,128)S(1)} %get-tuple-element.11.dw_ref), custom_call_target="tpu_custom_call" | custom-call | tf_op jit(solution)/shard_map/pallas_call | solution.py:479
